TPU v7x, 32 devices: a whole 2x2x4 slice. The times are simulated.
32 devices in a mesh: ep: 4 (over y, x), tp: 8 (over z, core).
Axes of the slice: x: 2, y: 2, z: 4, core: 2. Of those that a mesh axis runs over, the one named last changes fastest.
Arguments:
- queries: bfloat16 [4096, 1024], P('ep', 'tp'), may hold values from -600 to 600
- key_rows: bfloat16 [4096, 128], P('ep'), may hold values from -6 to 6
- value_rows: bfloat16 [4096, 128], P('ep'), may hold values from -48 to 48
- sink_logits: float32 [16], P('tp'), may hold values from 2 to 6
- out_weight: bfloat16 [1024, 2048], P('tp'), may hold values from -0.1875 to 0.1875
- moe_rows: bfloat16 [1024, 2048], P(('ep', 'tp')), may hold values from -6 to 6
- moe_gain: float32 [2048], replicated, may hold values from 0.1 to 1.9
- routes: int32 [1024, 2], P(('ep', 'tp')), may hold values from 0 to 3, all different within a row; in each aligned block of 32 rows (0 to 31, 32 to 63, ...) at most 24 rows name the same one
- route_weight: float32 [1024, 2], P(('ep', 'tp')), may hold values from 0.2 to 1
- gate_weight: bfloat16 [4, 2048, 7168], P('ep', None, 'tp'), may hold values from -0.125 to 0.125
- up_weight: bfloat16 [4, 2048, 7168], P('ep', None, 'tp'), may hold values from -0.125 to 0.125
- down_weight: bfloat16 [4, 7168, 2048], P('ep', 'tp'), may hold values from -0.0625 to 0.0625
Outputs:
- mixer_out: bfloat16 [4096, 2048], P(('ep', 'tp'))
- moe_out: bfloat16 [1024, 2048], P(('ep', 'tp'))
Inputs may be any that keep to these rules, and one draw needn't show every extreme that they name: `routes`: in each aligned block of 32 rows (the rows of one device) no expert is named more than 24 times, a bound that some block reaches; each row names 2 different experts.
All inputs are finite; a program needn't handle non-finite values.
Results may differ from a plain program's by a relative error of at most 0.02.
Values may be sent and summed in bfloat16 or wider, within the bound.
A program may use at most 128 MiB of HBM per device.

v0:
```python
import jax
import jax.numpy as jnp
from jax import lax
from jax.sharding import PartitionSpec as P

HEADS = 16
KV_HEADS = 2
HEAD_DIM = 64
WINDOW = 128
TOP = 2
big_negative = -1e30
norm_eps = 1e-05


def passed_along(value, axis, steps):
    count = lax.axis_size(axis)
    initial, last = (max(0, -steps), min(count, count - steps))
    return lax.ppermute(value, axis, [(source, source + steps) for source in range(initial, last)])


def layer_normed(inputs, gain):
    values = inputs.astype(jnp.float32)
    center = values - jnp.mean(values, -1, keepdims=True)
    spread = jnp.mean(center * center, -1, keepdims=True)
    return (center * lax.rsqrt(spread + norm_eps) * gain).astype(jnp.bfloat16)


def attend(queries, key_rows, value_rows, sink_logits):
    total = queries.shape[0]
    heads_here = sink_logits.shape[0]
    blocks = total // WINDOW
    key_head = lax.axis_index("tp") * heads_here // (HEADS // KV_HEADS)
    key_own = lax.dynamic_slice_in_dim(key_rows, key_head * HEAD_DIM, HEAD_DIM, 1)
    value_own = lax.dynamic_slice_in_dim(value_rows, key_head * HEAD_DIM, HEAD_DIM, 1)
    last_rows = jnp.concatenate([key_own[total - WINDOW :], value_own[total - WINDOW :]], 1)
    earlier = passed_along(last_rows, "ep", 1)
    key_ext = jnp.concatenate([earlier[:, :HEAD_DIM], key_own], 0)
    value_ext = jnp.concatenate([earlier[:, HEAD_DIM:], value_own], 0)
    key_blocks = jnp.concatenate(
        [
            key_ext[:total].reshape(blocks, WINDOW, HEAD_DIM),
            key_ext[WINDOW:].reshape(blocks, WINDOW, HEAD_DIM),
        ],
        1,
    )
    value_blocks = jnp.concatenate(
        [
            value_ext[:total].reshape(blocks, WINDOW, HEAD_DIM),
            value_ext[WINDOW:].reshape(blocks, WINDOW, HEAD_DIM),
        ],
        1,
    )
    query_blocks = queries.reshape(blocks, WINDOW, heads_here, HEAD_DIM)
    scores = jnp.einsum(
        "nqhd,nkd->nhqk", query_blocks, key_blocks, preferred_element_type=jnp.float32
    ) * HEAD_DIM ** (-0.5)
    anchor = lax.axis_index("ep") * total
    block_base = anchor + jnp.arange(blocks, dtype=jnp.int32)[:, None, None] * WINDOW
    query_pos = block_base + jnp.arange(WINDOW, dtype=jnp.int32)[None, :, None]
    key_pos = block_base - WINDOW + jnp.arange(2 * WINDOW, dtype=jnp.int32)[None, None, :]
    allowed = ((key_pos <= query_pos) & (key_pos > query_pos - WINDOW) & (key_pos >= 0))[:, None]
    masked = jnp.where(allowed, scores, big_negative)
    sinks = sink_logits[None, :, None]
    row_max = jnp.maximum(jnp.max(masked, -1), sinks)
    powers = jnp.where(allowed, jnp.exp(masked - row_max[..., None]), 0.0)
    totals = jnp.sum(powers, -1) + jnp.exp(sinks - row_max)
    attn_probs = (powers / totals[..., None]).astype(jnp.bfloat16)
    attended = jnp.einsum(
        "nhqk,nkd->nqhd", attn_probs, value_blocks, preferred_element_type=jnp.float32
    )
    return attended.astype(jnp.bfloat16).reshape(total, heads_here * HEAD_DIM)


def mixer(queries, key_rows, value_rows, sink_logits, out_weight):
    attended = attend(queries, key_rows, value_rows, sink_logits)
    return lax.psum_scatter(
        jnp.dot(attended, out_weight, preferred_element_type=jnp.float32).astype(jnp.bfloat16),
        "tp",
        scatter_dimension=0,
        tiled=True,
    )


def experts(moe_rows, moe_gain, routes, route_weight, gate_weight, up_weight, down_weight):
    row_count = moe_rows.shape[0]
    width_all = moe_rows.shape[1]
    expert_count = gate_weight.shape[0] * lax.axis_size("ep")
    capacity = 3 * row_count * TOP // (2 * expert_count)
    normed = layer_normed(moe_rows, moe_gain)
    chosen = routes.reshape(-1)
    onehot = (chosen[:, None] == jnp.arange(expert_count, dtype=jnp.int32)[None, :]).astype(
        jnp.int32
    )
    earlier_count = jnp.cumsum(onehot, 0) - onehot
    slot_index = jnp.sum(earlier_count * onehot, 1)
    target = chosen * capacity + slot_index
    matches = target[None, :] == jnp.arange(expert_count * capacity, dtype=jnp.int32)[:, None]
    dispatch_map = jnp.sum(matches.reshape(expert_count * capacity, row_count, TOP), -1).astype(
        jnp.bfloat16
    )
    buffer = jnp.dot(dispatch_map, normed, preferred_element_type=jnp.float32).astype(jnp.bfloat16)
    buffer = buffer.reshape(expert_count, capacity, width_all)
    gate_mat = gate_weight[0]
    up_mat = up_weight[0]
    down_mat = down_weight[0]
    received = lax.all_to_all(buffer, "ep", split_axis=0, concat_axis=0, tiled=True)
    total = received.shape[0] * received.shape[1]
    flat_rows = received.reshape(total, width_all)
    shard_rows = lax.all_gather(flat_rows, "tp", axis=0, tiled=True)
    gate_val = jnp.dot(shard_rows, gate_mat, preferred_element_type=jnp.float32)
    up_val = jnp.dot(shard_rows, up_mat, preferred_element_type=jnp.float32)
    hidden = (jax.nn.silu(gate_val) * up_val).astype(jnp.bfloat16)
    summed = lax.psum_scatter(
        jnp.dot(hidden, down_mat, preferred_element_type=jnp.float32).astype(jnp.bfloat16),
        "tp",
        scatter_dimension=0,
        tiled=True,
    )
    results = summed.reshape(received.shape)
    returned = lax.all_to_all(results, "ep", split_axis=0, concat_axis=0, tiled=True)
    weights_flat = route_weight.reshape(-1)
    combine_map = jnp.sum(
        jnp.where(matches, weights_flat[None, :], 0.0).reshape(
            expert_count * capacity, row_count, TOP
        ),
        -1,
    )
    returned_flat = returned.reshape(expert_count * capacity, width_all).astype(jnp.float32)
    moe_out = lax.dot_general(
        combine_map, returned_flat, (((0,), (0,)), ((), ())), precision=lax.Precision.HIGHEST
    )
    return moe_out.astype(jnp.bfloat16)


def dense_experts(moe_rows, moe_gain, routes, route_weight, gate_weight, up_weight, down_weight):
    count = lax.axis_size("ep")
    normed = layer_normed(moe_rows, moe_gain)
    both = ("ep", "tp")
    rows = lax.all_gather(normed, both, axis=0, tiled=True)
    named = routes[:, :, None] == jnp.arange(count, dtype=jnp.int32)[None, None, :]
    shares = jnp.sum(jnp.where(named, route_weight[:, :, None], 0.0), 1)
    shares = lax.all_gather(shares, both, axis=0, tiled=True)
    share = lax.dynamic_slice_in_dim(shares, lax.axis_index("ep"), 1, 1)
    gate_val = jnp.dot(rows, gate_weight[0], preferred_element_type=jnp.float32)
    up_val = jnp.dot(rows, up_weight[0], preferred_element_type=jnp.float32)
    hidden = (jax.nn.silu(gate_val) * up_val).astype(jnp.bfloat16)
    down = jnp.dot(hidden, down_weight[0], preferred_element_type=jnp.float32)
    return lax.psum_scatter(
        (down * share).astype(jnp.bfloat16), both, scatter_dimension=0, tiled=True
    )


def body(
    queries,
    key_rows,
    value_rows,
    sink_logits,
    out_weight,
    moe_rows,
    moe_gain,
    routes,
    route_weight,
    gate_weight,
    up_weight,
    down_weight,
):
    mixer_out = mixer(queries, key_rows, value_rows, sink_logits, out_weight)
    slots = 3 * moe_rows.shape[0] * TOP // 2
    sparse = (
        slots * lax.axis_size("tp")
        < moe_rows.shape[0] * lax.axis_size("tp") * lax.axis_size("ep") // 2
    )
    layer = experts if sparse else dense_experts
    moe_out = layer(moe_rows, moe_gain, routes, route_weight, gate_weight, up_weight, down_weight)
    return (mixer_out, moe_out)


def solution(mesh):
    in_specs = (
        P("ep", "tp"),
        P("ep", None),
        P("ep", None),
        P("tp"),
        P("tp", None),
        P(("ep", "tp"), None),
        P(),
        P(("ep", "tp"), None),
        P(("ep", "tp"), None),
        P("ep", None, "tp"),
        P("ep", None, "tp"),
        P("ep", "tp", None),
    )
    out_specs = (P(("ep", "tp"), None), P(("ep", "tp"), None))
    return jax.shard_map(body, mesh=mesh, in_specs=in_specs, out_specs=out_specs, check_vma=False)
```

profile of v0, /device:TPU:0, one launch (start us, length us, event | category | flops | bytes accessed | tf_op | source)
XLA Modules:
  0.0 265.6 jit_solution(14966716993027986457)
XLA Ops:
  8.0 0.0 copy-start
  8.0 0.0 all-gather.3.cloned.1.call-start
  8.1 1.1 convert_reduce_fusion
  9.1 1.1 fusion.14
  10.3 1.7 fusion.16
  11.9 0.0 all-gather.3.cloned.1.call-update
  12.0 0.0 reduce-scatter.3.cloned.1.call-start
  12.0 0.8 dynamic-slice
  12.9 0.8 dynamic-slice.1
  13.7 0.1 pad_maximum_fusion.2
  13.8 4.9 %collective-permute-start = (bf16[128,128]{1,0:T(8,128)(2,1)S(1)}, bf16[128,128]{1,0:T(8,128)(2,1)S(1)}, u32[]{:S(2)}, u32[]{:S(2)}) collective-permute-start(bf16[128,128]{1,0:T(8,128)(2,1)S(1)} %pad_maximum_fusion.2), channel_id=1, source_target_pairs={{0,8},{8,16},{16,24},{1,9},{9,17},{17,25},{2,10},{10,18},{18,26},{... | collective-permute-start | bytes 98312 | tf_op jit(solution)/shard_map/ppermute | solution.py:18
  18.7 0.1 broadcast_compare_fusion
  18.8 0.1 iota_add_fusion
  18.9 0.1 iota_add_fusion.1
  19.0 0.7 and_and_fusion
  19.7 1.2 constant_dynamic-slice_fusion.1
  20.9 0.0 copy-start.1
  20.9 0.1 copy.55
  21.1 0.1 copy.51
  21.2 1.2 reshape.156
  22.4 0.0 collective-permute-done
  22.4 0.1 fusion.28
  22.5 0.1 pad_maximum_fusion.1
  22.6 0.1 copy.50
  22.7 0.1 pad_maximum_fusion
  22.8 0.1 copy.54
  22.9 0.6 fusion.7
  23.5 0.0 copy-done.1
  23.5 0.1 broadcast_maximum_fusion
  23.6 0.6 fusion.8
  24.2 0.1 exponential_add_fusion
  24.3 0.7 fusion.9
  25.0 0.2 copy.59
  25.2 0.0 copy-done
  25.2 3.2 %convolution_convert_fusion = bf16[1024,2048]{1,0:T(8,128)(2,1)} fusion(bf16[128,2048]{1,0:T(8,128)(2,1)S(1)} %copy-done, bf16[16,8,8,128]{3,2,1,0:T(8,128)(2,1)S(1)} %bitcast.57), kind=kOutput, calls=%fused_computation.1 | convolution fusion | flops 538968064 | bytes 4980736 | tf_op jit(solution)/shard_map/dot_general | solution.py:77
  28.4 0.0 copy-start.2
  28.4 0.0 copy-start.3
  28.4 0.0 reduce-scatter.3.cloned.1.call-update
  28.4 0.0 reduce-scatter.5.cloned.1.call-start
  28.5 0.6 copy-done.2
  29.1 0.0 copy-done.3
  29.1 42.2 %all-gather = f32[32,32,4]{1,2,0:T(4,128)S(1)} all-gather(f32[1,32,4]{1,2,0:T(4,128)S(1)} %bitcast.60), channel_id=1, replica_groups=mesh['ep'=4,'tp'=8] {'ep','tp'}, dimensions={0}, use_global_device_ids=true | all-gather | bytes 16896 | tf_op jit(solution)/shard_map/all_gather | solution.py:142
  71.3 0.1 reshape.153
  71.4 25.5 %all-gather.3.cloned.1.call-done = bf16[1024,2048]{1,0:T(8,128)(2,1)} async-done(((bf16[32,2048]{1,0:T(8,128)(2,1)}), bf16[1024,2048]{1,0:T(8,128)(2,1)}) %all-gather.3.cloned.1.call-update) | async-done | bytes 4194320 | tf_op jit(solution)/shard_map/all_gather | solution.py:139
  97.0 0.0 copy-start.4
  97.0 0.0 copy-start.5
  97.0 7.5 %fusion.1 = f32[1024,896]{1,0:T(8,128)S(1)} fusion(bf16[1024,2048]{1,0:T(8,128)(2,1)} %all-gather.3.cloned.1.call-done, bf16[1,2048,896]{2,1,0:T(8,128)(2,1)} %param.22), kind=kOutput, calls=%fused_computation.3 | convolution fusion | flops 3758096384 | bytes 11534336 | tf_op jit(solution)/shard_map/dot_general | solution.py:145
  104.5 0.0 copy-done.4
  104.5 0.0 copy-done.5
  104.5 0.0 copy-start.6
  104.5 4.8 %multiply_convert_fusion.1 = bf16[1024,896]{1,0:T(8,128)(2,1)S(1)} fusion(f32[1024,896]{1,0:T(8,128)S(1)} %fusion.1, bf16[1024,2048]{1,0:T(8,128)(2,1)S(1)} %copy-done.4, bf16[1,2048,896]{2,1,0:T(8,128)(2,1)S(1)} %copy-done.5), kind=kOutput, calls=%fused_computation.7 | convolution fusion | flops 3763601408 | bytes 13369344 | tf_op jit(solution)/shard_map/dot_general | solution.py:144
  109.3 0.0 copy-done.6
  109.3 6.1 %multiply_convert_fusion = bf16[1024,2048]{1,0:T(8,128)(2,1)} fusion(bf16[1024,896]{1,0:T(8,128)(2,1)S(1)} %multiply_convert_fusion.1, f32[1024]{0:T(1024)S(1)} %bitcast.61, bf16[1,896,2048]{2,1,0:T(8,128)(2,1)S(1)} %copy-done.6), kind=kOutput, calls=%fused_computation | convolution fusion | flops 3762290688 | bytes 9703424 | tf_op jit(solution)/shard_map/dot_general | solution.py:147
  115.4 0.0 reduce-scatter.5.cloned.1.call-update
  115.4 0.0 reduce-scatter.3.cloned.1.call-done
  115.4 142.8 %reduce-scatter.5.cloned.1.call-done = bf16[32,2048]{1,0:T(8,128)(2,1)} async-done(((bf16[1024,2048]{1,0:T(8,128)(2,1)}), bf16[32,2048]{1,0:T(8,128)(2,1)}) %reduce-scatter.5.cloned.1.call-update) | async-done | bytes 131088 | tf_op jit(solution)/shard_map/reduce_scatter | solution.py:148
  (6 shorter events, 0.0 us)
Async XLA Ops:
  8.0 17.2 %copy-start = (bf16[128,2048]{1,0:T(8,128)(2,1)S(1)}, bf16[128,2048]{1,0:T(8,128)(2,1)}, u32[]{:S(2)}) copy-start(bf16[128,2048]{1,0:T(8,128)(2,1)} %param.16) | copy-start | bytes 1572868
  8.0 89.0 %all-gather.3.cloned.1.call-start = ((), (), s32[]{:S(2)}) async-start(), calls=%async_computation.3 | async-start | bytes 4325376 | tf_op jit(solution)/shard_map/all_gather | solution.py:139
  12.0 103.4 %reduce-scatter.3.cloned.1.call-start = ((), (), s32[]{:S(2)}) async-start(), calls=%async_computation.2 | async-start | bytes 4718592 | tf_op jit(solution)/shard_map/reduce_scatter | solution.py:76
  13.8 8.6 %collective-permute-start = (bf16[128,128]{1,0:T(8,128)(2,1)S(1)}, bf16[128,128]{1,0:T(8,128)(2,1)S(1)}, u32[]{:S(2)}, u32[]{:S(2)}) collective-permute-start(bf16[128,128]{1,0:T(8,128)(2,1)S(1)} %pad_maximum_fusion.2), channel_id=1, source_target_pairs={{0,8},{8,16},{16,24},{1,9},{9,17},{17,25},{2,10},{10,18},{18,26},{... | collective-permute-start | bytes 98312 | tf_op jit(solution)/shard_map/ppermute | solution.py:18
  20.9 2.6 copy-start.1
  28.4 0.7 copy-start.2
  28.4 0.7 copy-start.3
  28.4 229.8 %reduce-scatter.5.cloned.1.call-start = ((), (), s32[]{:S(2)}) async-start(), calls=%async_computation.4 | async-start | bytes 4325376 | tf_op jit(solution)/shard_map/reduce_scatter | solution.py:148
  97.0 7.5 %copy-start.4 = (bf16[1024,2048]{1,0:T(8,128)(2,1)S(1)}, bf16[1024,2048]{1,0:T(8,128)(2,1)}, u32[]{:S(2)}) copy-start(bf16[1024,2048]{1,0:T(8,128)(2,1)} %all-gather.3.cloned.1.call-done) | copy-start | bytes 12582916
  97.0 7.5 %copy-start.5 = (bf16[1,2048,896]{2,1,0:T(8,128)(2,1)S(1)}, bf16[1,2048,896]{2,1,0:T(8,128)(2,1)}, u32[]{:S(2)}) copy-start(bf16[1,2048,896]{2,1,0:T(8,128)(2,1)} %param.21) | copy-start | bytes 11010052
  104.5 4.8 %copy-start.6 = (bf16[1,896,2048]{2,1,0:T(8,128)(2,1)S(1)}, bf16[1,896,2048]{2,1,0:T(8,128)(2,1)}, u32[]{:S(2)}) copy-start(bf16[1,896,2048]{2,1,0:T(8,128)(2,1)} %param.23) | copy-start | bytes 11010052
Sparse Core Ops, SparseCore 0:
  12.4 84.5 all-gather.2
Sparse Core Ops, SparseCore 1:
  28.5 64.4 reduce-scatter.2
  115.5 142.7 reduce-scatter.4
where the time goes:
time: 266 us
  waiting for transfers between devices  168 us (63%)
  blocking collectives  42.2 us (16%)
  matrix products  22.9 us (9%)
  between operations  15.7 us (6%)
  other arithmetic  5.77 us (2%)
  local copies, waits for them, and re-layouts  5.72 us (2%)
  starting transfers between devices  5 us (2%)
    reduce_scatter x1, waiting for transfers between devices, dense_experts(): lax.psum_scatter((down * share).astype(jnp.bfloat16), both, scatter_dimen...  143 us
    all_gather x1, blocking collectives, dense_experts(): shares = lax.all_gather(shares, both, axis=0, tiled=True)  42.2 us
    all_gather x1, waiting for transfers between devices, dense_experts(): rows = lax.all_gather(normed, both, axis=0, tiled=True)  25.5 us
    dot_general x1, matrix products, dense_experts(): up_val = jnp.dot(rows, up_weight[0], preferred_element_type=jnp.float32)  7.49 us
    dot_general x1, matrix products, dense_experts(): down = jnp.dot(hidden, down_weight[0], preferred_element_type=jnp.float32)  6.08 us
  transfers between devices with their start and end apart: 4, of which 2 were waited for; matrix products, arithmetic and copies ran while one was open for 11% of the time, Pallas kernels for 0%

commit v1 on v0

--- a/solution.py
+++ b/solution.py
@@ -136,10 +136,13 @@
     count = lax.axis_size("ep")
     normed = layer_normed(moe_rows, moe_gain)
     both = ("ep", "tp")
-    rows = lax.all_gather(normed, both, axis=0, tiled=True)
     named = routes[:, :, None] == jnp.arange(count, dtype=jnp.int32)[None, None, :]
     shares = jnp.sum(jnp.where(named, route_weight[:, :, None], 0.0), 1)
-    shares = lax.all_gather(shares, both, axis=0, tiled=True)
+    rows, shares = jnp.split(
+        lax.all_gather(jnp.concatenate([normed, shares], axis=1), both, axis=0, tiled=True),
+        [normed.shape[1]],
+        axis=1,
+    )
     share = lax.dynamic_slice_in_dim(shares, lax.axis_index("ep"), 1, 1)
     gate_val = jnp.dot(rows, gate_weight[0], preferred_element_type=jnp.float32)
     up_val = jnp.dot(rows, up_weight[0], preferred_element_type=jnp.float32)

time: 266 us -> 288 us (1.083)
  waiting for transfers between devices: 168 us -> 231 us
  blocking collectives: 42.2 us -> 0 us
    all_gather x1, waiting for transfers between devices: 25.5 us -> 87.7 us  [dense_experts(): lax.all_gather(jnp.concatenate([normed, shares], axis=1), both, axis=0, t...]
    all_gather x1 -> x0, blocking collectives: 42.2 us -> none  [dense_experts(): shares = lax.all_gather(shares, both, axis=0, tiled=True)]
where the time goes in v1:
time: 288 us; the launch traced here: 287 us
  waiting for transfers between devices  231 us (80%)
  matrix products  23.6 us (8%)
  between operations  15.8 us (5%)
  other arithmetic  6.59 us (2%)
  local copies, waits for them, and re-layouts  5.58 us (2%)
  starting transfers between devices  5 us (2%)
    reduce_scatter x1, waiting for transfers between devices, dense_experts(): lax.psum_scatter((down * share).astype(jnp.bfloat16), both, scatter_dimen...  143 us
    all_gather x1, waiting for transfers between devices, dense_experts(): lax.all_gather(jnp.concatenate([normed, shares], axis=1), both, axis=0, t...  87.7 us
    dot_general x1, matrix products, dense_experts(): up_val = jnp.dot(rows, up_weight[0], preferred_element_type=jnp.float32)  8.19 us
    dot_general x1, matrix products, dense_experts(): down = jnp.dot(hidden, down_weight[0], preferred_element_type=jnp.float32)  6.04 us
  transfers between devices with their start and end apart: 4, of which 2 were waited for; matrix products, arithmetic and copies ran while one was open for 11% of the time, Pallas kernels for 0%

profile of v1, /device:TPU:0, one launch (start us, length us, event | category | flops | bytes accessed | tf_op | source)
XLA Modules:
  0.0 287.5 jit_solution(13802841040865803329)
XLA Ops:
  8.0 0.0 copy-start
  8.0 0.0 copy-start.1
  8.0 0.0 all-gather.2.cloned.1.call-start
  8.1 1.1 convert_reduce_fusion
  9.2 1.1 fusion.18
  10.3 0.7 select_reduce_fusion
  11.0 0.1 copy.44
  11.1 1.0 fusion.27
  12.1 0.8 pad_maximum_fusion
  12.9 0.0 all-gather.2.cloned.1.call-update
  12.9 0.0 reduce-scatter.3.cloned.1.call-start
  13.0 0.8 dynamic-slice
  13.8 0.8 dynamic-slice.1
  14.7 0.1 pad_maximum_fusion.3
  14.8 4.9 %collective-permute-start = (bf16[128,128]{1,0:T(8,128)(2,1)S(1)}, bf16[128,128]{1,0:T(8,128)(2,1)S(1)}, u32[]{:S(2)}, u32[]{:S(2)}) collective-permute-start(bf16[128,128]{1,0:T(8,128)(2,1)S(1)} %pad_maximum_fusion.3), channel_id=1, source_target_pairs={{0,8},{8,16},{16,24},{1,9},{9,17},{17,25},{2,10},{10,18},{18,26},{... | collective-permute-start | bytes 98312 | tf_op jit(solution)/shard_map/ppermute | solution.py:18
  19.7 0.1 broadcast_compare_fusion
  19.7 0.1 iota_add_fusion
  19.8 0.1 iota_add_fusion.1
  19.9 0.7 and_and_fusion
  20.6 1.2 constant_dynamic-slice_fusion
  21.9 0.0 copy-start.2
  21.9 0.1 copy.39
  22.0 0.1 copy.35
  22.2 0.0 copy-done.1
  22.2 0.2 reshape.154
  22.4 0.0 collective-permute-done
  22.4 0.1 fusion.33
  22.5 0.1 pad_maximum_fusion.2
  22.6 0.1 copy.34
  22.7 0.1 pad_maximum_fusion.1
  22.8 0.1 copy.38
  22.9 0.6 fusion.11
  23.5 0.0 copy-done.2
  23.5 0.1 broadcast_maximum_fusion
  23.6 0.6 fusion.12
  24.2 0.1 exponential_add_fusion
  24.2 0.7 fusion.13
  25.0 0.2 copy.43
  25.2 0.0 copy-done
  25.2 3.3 %convolution_convert_fusion = bf16[1024,2048]{1,0:T(8,128)(2,1)} fusion(bf16[128,2048]{1,0:T(8,128)(2,1)S(1)} %copy-done, bf16[16,8,8,128]{3,2,1,0:T(8,128)(2,1)S(1)} %bitcast.51), kind=kOutput, calls=%fused_computation.5 | convolution fusion | flops 538968064 | bytes 4980736 | tf_op jit(solution)/shard_map/dot_general | solution.py:77
  28.4 0.0 reduce-scatter.3.cloned.1.call-update
  28.5 0.0 reduce-scatter.5.cloned.1.call-start
  28.5 87.7 %all-gather.2.cloned.1.call-done = f32[1024,2052]{1,0:T(8,128)} async-done(((f32[32,2052]{1,0:T(8,128)}), f32[1024,2052]{1,0:T(8,128)}) %all-gather.2.cloned.1.call-update) | async-done | bytes 8405008 | tf_op jit(solution)/shard_map/all_gather | solution.py:142
  116.2 1.1 split.9
  117.3 0.0 slice-start
  117.3 0.4 dynamic-slice_reduce_fusion
  117.7 0.0 slice-start.1
  117.7 0.0 slice-start.2
  117.7 0.0 copy-start.3
  117.7 8.2 %fusion = f32[1024,896]{1,0:T(8,128)S(1)} fusion(f32[1024,2052]{1,0:T(8,128)} %all-gather.2.cloned.1.call-done, bf16[1,2048,896]{2,1,0:T(8,128)(2,1)} %param.22), kind=kOutput, calls=%fused_computation.1 | convolution fusion | flops 3758096384 | bytes 11534336 | tf_op jit(solution)/shard_map/dot_general | solution.py:148
  125.9 0.0 slice-done
  125.9 0.0 slice-done.1
  125.9 0.0 slice-done.2
  125.9 0.0 copy-done.3
  125.9 0.0 copy-start.4
  125.9 4.8 %multiply_convert_fusion.1 = bf16[1024,896]{1,0:T(8,128)(2,1)S(1)} fusion(f32[1024,896]{1,0:T(8,128)S(1)} %fusion, bf16[1,2048,896]{2,1,0:T(8,128)(2,1)S(1)} %copy-done.3, f32[1024,2052]{1,0:T(8,128)S(1)} %bitcast.55), kind=kOutput, calls=%fused_computation.9 | convolution fusion | flops 3763601408 | bytes 13369344 | tf_op jit(solution)/shard_map/dot_general | solution.py:147
  130.8 0.0 copy-done.4
  130.8 6.0 %multiply_convert_fusion = bf16[1024,2048]{1,0:T(8,128)(2,1)} fusion(bf16[1024,896]{1,0:T(8,128)(2,1)S(1)} %multiply_convert_fusion.1, f32[1024]{0:T(1024)S(1)} %dynamic-slice_reduce_fusion, bf16[1,896,2048]{2,1,0:T(8,128)(2,1)S(1)} %copy-done.4), kind=kOutput, calls=%fused_computation | convolution fusion | flops 3762290688 | bytes 9703424 | tf_op jit(solution)/shard_map/dot_general | solution.py:150
  136.8 0.0 reduce-scatter.5.cloned.1.call-update
  136.8 0.0 reduce-scatter.3.cloned.1.call-done
  136.9 143.2 %reduce-scatter.5.cloned.1.call-done = bf16[32,2048]{1,0:T(8,128)(2,1)} async-done(((bf16[1024,2048]{1,0:T(8,128)(2,1)}), bf16[32,2048]{1,0:T(8,128)(2,1)}) %reduce-scatter.5.cloned.1.call-update) | async-done | bytes 131088 | tf_op jit(solution)/shard_map/reduce_scatter | solution.py:151
  (4 shorter events, 0.0 us)
Async XLA Ops:
  8.0 17.2 %copy-start = (bf16[128,2048]{1,0:T(8,128)(2,1)S(1)}, bf16[128,2048]{1,0:T(8,128)(2,1)}, u32[]{:S(2)}) copy-start(bf16[128,2048]{1,0:T(8,128)(2,1)} %param.16) | copy-start | bytes 1572868
  8.0 14.2 %copy-start.1 = (bf16[1024,128]{1,0:T(8,128)(2,1)S(1)}, bf16[1024,128]{1,0:T(8,128)(2,1)}, u32[]{:S(2)}) copy-start(bf16[1024,128]{1,0:T(8,128)(2,1)} %param.12) | copy-start | bytes 786436
  8.0 108.2 %all-gather.2.cloned.1.call-start = ((), (), s32[]{:S(2)}) async-start(), calls=%async_computation.3 | async-start | bytes 9191424 | tf_op jit(solution)/shard_map/all_gather | solution.py:142
  12.9 123.9 %reduce-scatter.3.cloned.1.call-start = ((), (), s32[]{:S(2)}) async-start(), calls=%async_computation.2 | async-start | bytes 4718592 | tf_op jit(solution)/shard_map/reduce_scatter | solution.py:76
  14.8 7.7 %collective-permute-start = (bf16[128,128]{1,0:T(8,128)(2,1)S(1)}, bf16[128,128]{1,0:T(8,128)(2,1)S(1)}, u32[]{:S(2)}, u32[]{:S(2)}) collective-permute-start(bf16[128,128]{1,0:T(8,128)(2,1)S(1)} %pad_maximum_fusion.3), channel_id=1, source_target_pairs={{0,8},{8,16},{16,24},{1,9},{9,17},{17,25},{2,10},{10,18},{18,26},{... | collective-permute-start | bytes 98312 | tf_op jit(solution)/shard_map/ppermute | solution.py:18
  21.9 1.6 copy-start.2
  28.5 251.6 %reduce-scatter.5.cloned.1.call-start = ((), (), s32[]{:S(2)}) async-start(), calls=%async_computation.4 | async-start | bytes 4325376 | tf_op jit(solution)/shard_map/reduce_scatter | solution.py:151
  117.3 8.6 %slice-start = ((s8[8912896]{0:T(1024)(128)(4,1)}), s8[4194304]{0:T(1024)(128)(4,1)S(1)}, s32[]{:S(2)}) async-start(s8[8912896]{0:T(1024)(128)(4,1)} %bitcast.54), calls=%async_computation.5 | async-start | bytes 8388608
  117.7 8.2 %slice-start.1 = ((s8[8912896]{0:T(1024)(128)(4,1)}), s8[4194304]{0:T(1024)(128)(4,1)S(1)}, s32[]{:S(2)}) async-start(s8[8912896]{0:T(1024)(128)(4,1)} %bitcast.54), calls=%async_computation.6 | async-start | bytes 8388608
  117.7 8.2 %slice-start.2 = ((s8[8912896]{0:T(1024)(128)(4,1)}), s8[524288]{0:T(1024)(128)(4,1)S(1)}, s32[]{:S(2)}) async-start(s8[8912896]{0:T(1024)(128)(4,1)} %bitcast.54), calls=%async_computation.7 | async-start | bytes 1048576
  117.7 8.2 %copy-start.3 = (bf16[1,2048,896]{2,1,0:T(8,128)(2,1)S(1)}, bf16[1,2048,896]{2,1,0:T(8,128)(2,1)}, u32[]{:S(2)}) copy-start(bf16[1,2048,896]{2,1,0:T(8,128)(2,1)} %param.21) | copy-start | bytes 11010052
  125.9 4.8 %copy-start.4 = (bf16[1,896,2048]{2,1,0:T(8,128)(2,1)S(1)}, bf16[1,896,2048]{2,1,0:T(8,128)(2,1)}, u32[]{:S(2)}) copy-start(bf16[1,896,2048]{2,1,0:T(8,128)(2,1)} %param.23) | copy-start | bytes 11010052
Sparse Core Ops, SparseCore 0:
  13.0 103.1 all-gather.1
Sparse Core Ops, SparseCore 1:
  28.6 76.8 reduce-scatter.2
  136.9 143.1 reduce-scatter.4
